TPU v7x, 32 devices: a whole 2x2x4 slice. The times are simulated.
32 devices in a mesh: sp: 8 (over z, x), tp: 4 (over y, core).
Axes of the slice: x: 2, y: 2, z: 4, core: 2. Of those that a mesh axis runs over, the one named last changes fastest.
Arguments:
- lane_source_signal: bfloat16 [1024, 1024], P('tp', 'sp'), may hold values from -6 to 6
- spectral_damping_part: float32 [64, 64], P('tp'), may hold values from -3 to -0.0002
- spectral_angular_part: float32 [64, 64], P('tp'), may hold values from 0.31 to 201.0624
- interval_exponent: float32 [64], P('tp'), may hold values from -3.9 to -1.6
- entry_matrix_inphase: float32 [64, 64, 16], P('tp'), may hold values from -1 to 1
- entry_matrix_quadrature: float32 [64, 64, 16], P('tp'), may hold values from -1 to 1
- emission_inphase: float32 [64, 16, 64], P('tp'), may hold values from -0.75 to 0.75
- emission_quadrature: float32 [64, 16, 64], P('tp'), may hold values from -0.75 to 0.75
- lane_bypass_factor: float32 [1024], P('tp'), may hold values from -5 to 5
- spike_shrink_offset: float32 [64, 1024], P('tp', 'sp'), may hold values from -1.4 to 0
- lane_exit_matrix: bfloat16 [1024, 4096], P('tp'), may hold values from -0.1875 to 0.1875
- skipline_stream: bfloat16 [1024, 4096], P('sp'), may hold values from -6 to 6
- specialist_scaling_vector: float32 [4096], replicated, may hold values from 0.1 to 1.9
- selected_specialists: int32 [1024, 2], P('sp'), may hold values from 0 to 7, all different within a row; in each aligned block of 128 rows (0 to 127, 128 to 255, ...) at most 64 rows name the same one
- dispatcher_scores: float32 [1024, 2], P('sp'), may hold values from 0.1 to 1
- specialist_valve_matrix: bfloat16 [8, 4096, 2048], P('sp', None, 'tp'), may hold values from -0.09375 to 0.09375
- specialist_widen_matrix: bfloat16 [8, 4096, 2048], P('sp', None, 'tp'), may hold values from -0.09375 to 0.09375
- specialist_shrink_matrix: bfloat16 [8, 2048, 4096], P('sp', 'tp'), may hold values from -0.1875 to 0.1875
Outputs:
- updated: bfloat16 [1024, 4096], P('sp', 'tp')
Inputs may be any that keep to these rules, and one draw needn't show every extreme that they name: `selected_specialists`: each row names 2 different experts. Among the rows of each aligned block of 128 positions no expert is named more than 64 times, and in every block some expert is named exactly 64 times.
All inputs are finite; a program needn't handle non-finite values.
Results may differ from a plain program's by a relative error of at most 0.019.
Values may be sent and summed in bfloat16 or wider, within the bound.
No kernel may reach another device: no remote copies, remote signals or barrier semaphores. Data moves between devices by JAX's collectives and lax.ppermute only.
A program may use at most 64 MiB of HBM per device.

v0:
```python
import jax
import jax.numpy as jnp
from jax import lax
from jax.sharding import PartitionSpec as P

EPS = 1e-06
PRECISE_MODE = lax.Precision.HIGHEST


def carried_in(value, axis, join, neutral):
    count, mine = (lax.axis_size(axis), lax.axis_index(axis))
    pieces = jax.tree.map(lambda part: lax.all_gather(part, axis), value)
    running = jax.tree.map(
        lambda part, zero: jnp.full_like(part, 0) + jnp.asarray(zero, part.dtype), value, neutral
    )

    def lap(position, running):
        longer = join(running, jax.tree.map(lambda part: part[position], pieces))
        return jax.tree.map(lambda new, old: jnp.where(position < mine, new, old), longer, running)

    return lax.fori_loop(0, count - 1, lap, running)


def affine_pair(earlier, latter):
    mul_re = earlier[0] * latter[0] - earlier[1] * latter[1]
    mul_im = earlier[0] * latter[1] + earlier[1] * latter[0]
    add_re = latter[0] * earlier[2] - latter[1] * earlier[3] + latter[2]
    add_im = latter[0] * earlier[3] + latter[1] * earlier[2] + latter[3]
    return (mul_re, mul_im, add_re, add_im)


def local_prefix(elements):
    length = elements[0].shape[2]
    fills = (1.0, 0.0, 0.0, 0.0)
    offset = 1
    while offset < length:
        earlier = tuple(
            (
                jnp.pad(
                    item[:, :, : length - offset],
                    ((0, 0), (0, 0), (offset, 0)),
                    constant_values=fill,
                )
                for item, fill in zip(elements, fills)
            )
        )
        elements = affine_pair(earlier, elements)
        offset = offset * 2
    return elements


def full_norm(projected, skipline_stream, specialist_scaling_vector, col_start, d_local):
    stream = (
        skipline_stream.astype(jnp.float32)
        + lax.optimization_barrier(projected).astype(jnp.float32)
    ).astype(jnp.bfloat16)
    stream_f = lax.optimization_barrier(stream).astype(jnp.float32)
    inv_rms = lax.rsqrt(jnp.mean(stream_f * stream_f, axis=-1, keepdims=True) + EPS)
    normed = (stream_f * inv_rms * specialist_scaling_vector).astype(jnp.bfloat16)
    own_stream = lax.dynamic_slice_in_dim(stream_f, col_start, d_local, 1)
    own_cols = lax.dynamic_slice_in_dim(normed, col_start, d_local, 1)
    return (own_stream, normed, own_cols)


def per_device(
    lane_source_signal,
    spectral_damping_part,
    spectral_angular_part,
    interval_exponent,
    entry_matrix_inphase,
    entry_matrix_quadrature,
    emission_inphase,
    emission_quadrature,
    lane_bypass_factor,
    spike_shrink_offset,
    lane_exit_matrix,
    skipline_stream,
    specialist_scaling_vector,
    selected_specialists,
    dispatcher_scores,
    specialist_valve_matrix,
    specialist_widen_matrix,
    specialist_shrink_matrix,
):
    f32 = jnp.float32
    bf16 = jnp.bfloat16
    groups_here = spectral_damping_part.shape[0]
    lanes_within_bundle = entry_matrix_inphase.shape[2]
    tok_local = lane_source_signal.shape[1]
    bundled_signal = lane_source_signal.astype(f32).reshape(
        groups_here, lanes_within_bundle, tok_local
    )
    step_size = jnp.exp(interval_exponent)[:, None]
    natural_pace_exponent = spectral_damping_part * step_size
    angle = spectral_angular_part * step_size
    num_re = jnp.expm1(natural_pace_exponent) * jnp.cos(angle) - 2.0 * jnp.sin(0.5 * angle) ** 2
    num_im = jnp.exp(natural_pace_exponent) * jnp.sin(angle)
    denom = (
        spectral_damping_part * spectral_damping_part
        + spectral_angular_part * spectral_angular_part
    )
    fac_re = (num_re * spectral_damping_part + num_im * spectral_angular_part) / denom
    fac_im = (num_im * spectral_damping_part - num_re * spectral_angular_part) / denom
    map_re = (
        fac_re[:, :, None] * entry_matrix_inphase - fac_im[:, :, None] * entry_matrix_quadrature
    )
    map_im = (
        fac_re[:, :, None] * entry_matrix_quadrature + fac_im[:, :, None] * entry_matrix_inphase
    )
    drive_re = jnp.einsum("gpc,gct->gpt", map_re, bundled_signal, precision=PRECISE_MODE)
    drive_im = jnp.einsum("gpc,gct->gpt", map_im, bundled_signal, precision=PRECISE_MODE)
    recurrence_modulus = jnp.exp(
        natural_pace_exponent[:, :, None] + spike_shrink_offset[:, None, :]
    )
    trans_re = recurrence_modulus * jnp.cos(angle)[:, :, None]
    trans_im = recurrence_modulus * jnp.sin(angle)[:, :, None]
    cum_re, cum_im, state_real, state_imaginary = local_prefix(
        (trans_re, trans_im, drive_re, drive_im)
    )
    summary = (cum_re[:, :, -1], cum_im[:, :, -1], state_real[:, :, -1], state_imaginary[:, :, -1])
    unit = jnp.ones_like(summary[0])
    blank = jnp.zeros_like(summary[0])
    carried = carried_in(summary, "sp", affine_pair, (unit, blank, blank, blank))
    enter_re = carried[2][:, :, None]
    enter_im = carried[3][:, :, None]
    state_real = state_real + cum_re * enter_re - cum_im * enter_im
    state_imaginary = state_imaginary + cum_re * enter_im + cum_im * enter_re
    value = (
        jnp.einsum("nef,nfi->nei", emission_inphase, state_real, precision=PRECISE_MODE)
        - jnp.einsum("nef,nfi->nei", emission_quadrature, state_imaginary, precision=PRECISE_MODE)
        + lane_bypass_factor.reshape(groups_here, lanes_within_bundle)[:, :, None] * bundled_signal
    )
    recurrence_result = (
        jax.nn.gelu(value).astype(bf16).reshape(groups_here * lanes_within_bundle, tok_local)
    )
    width = specialist_scaling_vector.shape[0]
    d_local = width // lax.axis_size("tp")
    col_start = lax.axis_index("tp") * d_local
    partial_rows = jnp.einsum(
        "ct,cd->td", recurrence_result, lane_exit_matrix, preferred_element_type=f32
    )
    projected = lax.psum(partial_rows.astype(jnp.bfloat16), "tp").astype(jnp.float32).astype(bf16)
    own_stream, normed, own_cols = full_norm(
        projected, skipline_stream, specialist_scaling_vector, col_start, d_local
    )
    share = dispatcher_scores / jnp.sum(dispatcher_scores, axis=1, keepdims=True)
    experts = lax.axis_size("sp")
    top = selected_specialists.shape[1]
    capacity = 2 * tok_local * top // experts
    flat_routes = selected_specialists.reshape(-1)
    hits = (flat_routes[:, None] == jnp.arange(experts, dtype=jnp.int32)[None, :]).astype(jnp.int32)
    ranks = jnp.sum((jnp.cumsum(hits, axis=0) - hits) * hits, axis=1)
    slot_ids = flat_routes * capacity + ranks
    slot_grid = jnp.arange(experts * capacity, dtype=jnp.int32)
    matched = slot_grid[:, None] == slot_ids[None, :]
    token_of = jnp.arange(tok_local * top, dtype=jnp.int32) // top
    slot_token = jnp.sum(jnp.where(matched, token_of[None, :], 0), axis=1)
    slot_live = jnp.any(matched, axis=1)
    gate_w = specialist_valve_matrix[0]
    up_w = specialist_widen_matrix[0]
    down_w = specialist_shrink_matrix[0]
    bf_zero = jnp.zeros((), bf16)
    dispatch = jnp.where(slot_live[:, None], own_cols[slot_token], bf_zero).reshape(
        experts, capacity, d_local
    )
    arrived = lax.all_to_all(dispatch, "sp", split_axis=0, concat_axis=0, tiled=True)
    piece = lax.all_gather(arrived, "tp", axis=2, tiled=True)
    gate_part = jnp.einsum("snd,df->snf", piece, gate_w, preferred_element_type=f32)
    up_part = jnp.einsum("snd,df->snf", piece, up_w, preferred_element_type=f32)
    hidden = (jax.nn.silu(gate_part) * up_part).astype(bf16)
    flat_hidden = hidden.reshape(experts * capacity, hidden.shape[2])
    down_part = jnp.dot(flat_hidden, down_w, preferred_element_type=f32).astype(bf16)
    summed = lax.psum_scatter(
        down_part.astype(f32).astype(jnp.bfloat16), "tp", scatter_dimension=1, tiled=True
    ).astype(jnp.float32)
    expert_out = summed.astype(bf16).reshape(experts, capacity, d_local)
    returned = lax.all_to_all(expert_out, "sp", split_axis=0, concat_axis=0, tiled=True).reshape(
        experts * capacity, d_local
    )
    picked = returned[slot_ids].reshape(tok_local, top, d_local)
    combined = jnp.sum(lax.optimization_barrier(picked).astype(f32) * share[:, :, None], axis=1)
    return (own_stream + combined).astype(bf16)


def solution(mesh):
    placed = (
        P("tp", "sp"),
        P("tp", None),
        P("tp", None),
        P("tp"),
        P("tp", None, None),
        P("tp", None, None),
        P("tp", None, None),
        P("tp", None, None),
        P("tp"),
        P("tp", "sp"),
        P("tp", None),
        P("sp", None),
        P(),
        P("sp", None),
        P("sp", None),
        P("sp", None, "tp"),
        P("sp", None, "tp"),
        P("sp", "tp", None),
    )
    return jax.shard_map(
        per_device, mesh=mesh, in_specs=placed, out_specs=P("sp", "tp"), check_vma=False
    )
```

profile of v0, /device:TPU:0, one launch (start us, length us, event | category | flops | bytes accessed | tf_op | source)
XLA Modules:
  0.0 370.3 jit_solution(14271177628407040252)
XLA Ops:
  8.2 1.6 fusion.45
  9.8 1.6 fusion.49
  23.2 32.4 %all-gather = f32[128,64,1]{1,2,0:T(1,128)S(1)} all-gather(f32[16,64,1]{1,2,0:T(1,128)S(1)} %copy.32), channel_id=2, replica_groups=mesh['sp'=8,'tp'=4] {'sp'}, dimensions={0}, use_global_device_ids=true | all-gather | bytes 36864 | tf_op jit(solution)/shard_map/all_gather | solution.py:12
  57.8 30.5 %all-gather.1 = f32[128,64,1]{1,2,0:T(1,128)S(1)} all-gather(f32[16,64,1]{1,2,0:T(1,128)S(1)} %copy.33), channel_id=3, replica_groups=mesh['sp'=8,'tp'=4] {'sp'}, dimensions={0}, use_global_device_ids=true | all-gather | bytes 36864 | tf_op jit(solution)/shard_map/all_gather | solution.py:12
  88.3 2.0 slice.170
  91.6 30.5 %all-gather.2 = f32[128,64,1]{1,2,0:T(1,128)S(1)} all-gather(f32[16,64,1]{1,2,0:T(1,128)S(1)} %copy.34), channel_id=4, replica_groups=mesh['sp'=8,'tp'=4] {'sp'}, dimensions={0}, use_global_device_ids=true | all-gather | bytes 36864 | tf_op jit(solution)/shard_map/all_gather | solution.py:12
  122.2 2.0 slice.171
  125.4 30.5 %all-gather.3 = f32[128,64,1]{1,2,0:T(1,128)S(1)} all-gather(f32[16,64,1]{1,2,0:T(1,128)S(1)} %copy.35), channel_id=5, replica_groups=mesh['sp'=8,'tp'=4] {'sp'}, dimensions={0}, use_global_device_ids=true | all-gather | bytes 36864 | tf_op jit(solution)/shard_map/all_gather | solution.py:12
  156.4 1.9 fusion.22
  158.2 1.9 fusion.42
  160.1 1.5 convolution_convert_fusion.1
  163.7 35.4 %all-reduce.30.cloned.1.call-done = bf16[128,4096]{1,0:T(8,128)(2,1)} async-done(((bf16[128,4096]{1,0:T(8,128)(2,1)}), bf16[128,4096]{1,0:T(8,128)(2,1)}) %all-reduce.30.cloned.1.call-update) | async-done | bytes 1048592 | tf_op jit(solution)/shard_map/psum | solution.py:142
  199.0 1.8 add_convert_fusion
  202.5 2.1 gather_fusion
  204.7 30.6 %all_to_all.10 = bf16[8,64,1024]{2,1,0:T(8,128)(2,1)} all-to-all(bf16[8,64,1024]{2,1,0:T(8,128)(2,1)S(1)} %broadcast_select_fusion), channel_id=1, replica_groups=mesh['sp'=8,'tp'=4] {'sp'}, dimensions={0} | all-to-all | bytes 2097152 | tf_op jit(solution)/shard_map/all_to_all | solution.py:166
  235.4 33.4 %all-gather.6.cloned.1.call-done = bf16[8,64,4096]{2,1,0:T(8,128)(2,1)} async-done(((bf16[8,64,1024]{2,1,0:T(8,128)(2,1)}), bf16[8,64,4096]{2,1,0:T(8,128)(2,1)}) %all-gather.6.cloned.1.call-update) | async-done | bytes 4194320 | tf_op jit(solution)/shard_map/all_gather | solution.py:167
  268.9 5.9 %fusion.7 = f32[8,64,512]{2,1,0:T(8,128)S(1)} fusion(bf16[8,64,4096]{2,1,0:T(8,128)(2,1)} %all-gather.6.cloned.1.call-done, bf16[1,4096,512]{2,1,0:T(8,128)(2,1)} %param.35), kind=kOutput, calls=%fused_computation.17 | convolution fusion | flops 2147483648 | bytes 9437184 | tf_op jit(solution)/shard_map/snd,df->snf/dot_general | solution.py:168
  274.8 2.4 fusion.12
  277.3 4.3 %convolution_convert_fusion = bf16[512,4096]{1,0:T(8,128)(2,1)} fusion(bf16[512,512]{1,0:T(8,128)(2,1)S(1)} %bitcast.169, bf16[1,512,4096]{2,1,0:T(8,128)(2,1)S(1)} %copy-done.8), kind=kOutput, calls=%fused_computation.12 | convolution fusion | flops 2149580800 | bytes 8912896 | tf_op jit(solution)/shard_map/dot_general | solution.py:172
  281.6 44.6 %reduce-scatter.2.cloned.1.call-done = bf16[512,1024]{1,0:T(8,128)(2,1)} async-done(((bf16[512,4096]{1,0:T(8,128)(2,1)}), bf16[512,1024]{1,0:T(8,128)(2,1)}) %reduce-scatter.2.cloned.1.call-update) | async-done | bytes 1048592 | tf_op jit(solution)/shard_map/reduce_scatter | solution.py:173
  326.1 5.5 %all-to-all-start.1 = ((bf16[8,64,1024]{2,1,0:T(8,128)(2,1)}), bf16[8,64,1024]{2,1,0:T(8,128)(2,1)S(1)}, u32[]{:S(2)}, u32[]{:S(2)}) async-start(bf16[8,64,1024]{2,1,0:T(8,128)(2,1)} %bitcast.156), calls=%async_computation.2 | async-start | bytes 2097152 | tf_op jit(solution)/shard_map/all_to_all | solution.py:177
  332.1 25.2 %all-to-all-done.1 = bf16[8,64,1024]{2,1,0:T(8,128)(2,1)S(1)} async-done(((bf16[8,64,1024]{2,1,0:T(8,128)(2,1)}), bf16[8,64,1024]{2,1,0:T(8,128)(2,1)S(1)}, u32[]{:S(2)}, u32[]{:S(2)}) %all-to-all-start.1) | async-done | bytes 1048608 | tf_op jit(solution)/shard_map/all_to_all | solution.py:177
  357.3 2.0 gather_fusion.1
  361.9 1.8 add_convert_fusion.1
  (90 shorter events, 25.5 us)
Async XLA Ops:
  6.5 153.6 %copy-start = (bf16[256,4096]{1,0:T(8,128)(2,1)S(1)}, bf16[256,4096]{1,0:T(8,128)(2,1)}, u32[]{:S(2)}) copy-start(bf16[256,4096]{1,0:T(8,128)(2,1)} %param.30) | copy-start | bytes 6291460
  6.5 6.3 %copy-start.3 = (f32[16,128]{1,0:T(8,128)S(1)}, f32[16,128]{1,0:T(8,128)}, u32[]{:S(2)}) copy-start(f32[16,128]{1,0:T(8,128)} %param.29) | copy-start | bytes 24580
  6.5 192.5 %all-reduce.30.cloned.1.call-start = ((), (), s32[]{:S(2)}) async-start(), calls=%async_computation.3 | async-start | bytes 2097152 | tf_op jit(solution)/shard_map/psum | solution.py:142
  20.9 135.3 %copy-start.6 = (f32[256]{0:T(256)S(1)}, f32[256]{0:T(256)}, u32[]{:S(2)}) copy-start(f32[256]{0:T(256)} %param.28) | copy-start | bytes 3076
  21.9 136.3 %copy-start.2 = (bf16[256,128]{1,0:T(8,128)(2,1)S(1)}, bf16[256,128]{1,0:T(8,128)(2,1)}, u32[]{:S(2)}) copy-start(bf16[256,128]{1,0:T(8,128)(2,1)} %param.20) | copy-start | bytes 196612
  156.3 5.6 %copy-start.4 = (s32[128,2]{0,1:T(2,128)S(1)}, s32[128,2]{0,1:T(2,128)}, u32[]{:S(2)}) copy-start(s32[128,2]{0,1:T(2,128)} %param.33) | copy-start | bytes 3076
  161.6 107.2 %all-gather.6.cloned.1.call-start = ((), (), s32[]{:S(2)}) async-start(), calls=%async_computation.4 | async-start | bytes 5242880 | tf_op jit(solution)/shard_map/all_gather | solution.py:167
  163.5 38.9 %dynamic-slice-start = ((f32[4096]{0:T(1024)}, s32[]{:T(128)}), f32[1024]{0:T(1024)S(1)}, s32[]{:S(2)}) async-start(f32[4096]{0:T(1024)} %param.32, s32[]{:T(128)} %select_n.74), calls=%async_computation.6 | async-start | bytes 8704 | tf_op jit(solution)/shard_map/dynamic_slice | solution.py:61
  201.0 1.3 copy-start.1
  235.4 90.8 %reduce-scatter.2.cloned.1.call-start = ((), (), s32[]{:S(2)}) async-start(), calls=%async_computation.5 | async-start | bytes 5242880 | tf_op jit(solution)/shard_map/reduce_scatter | solution.py:173
  268.8 5.9 %copy-start.7 = (bf16[1,4096,512]{2,1,0:T(8,128)(2,1)S(1)}, bf16[1,4096,512]{2,1,0:T(8,128)(2,1)}, u32[]{:S(2)}) copy-start(bf16[1,4096,512]{2,1,0:T(8,128)(2,1)} %param.36) | copy-start | bytes 12582916
  268.9 5.9 %copy-start.9 = (bf16[8,64,4096]{2,1,0:T(8,128)(2,1)S(1)}, bf16[8,64,4096]{2,1,0:T(8,128)(2,1)}, u32[]{:S(2)}) copy-start(bf16[8,64,4096]{2,1,0:T(8,128)(2,1)} %all-gather.6.cloned.1.call-done) | copy-start | bytes 12582916
  274.8 2.5 copy-start.8
  281.6 50.4 %copy-start.5 = (f32[128,2]{0,1:T(2,128)S(1)}, f32[128,2]{0,1:T(2,128)}, u32[]{:S(2)}) copy-start(f32[128,2]{0,1:T(2,128)} %param.34) | copy-start | bytes 3076
  326.1 31.2 %all-to-all-start.1 = ((bf16[8,64,1024]{2,1,0:T(8,128)(2,1)}), bf16[8,64,1024]{2,1,0:T(8,128)(2,1)S(1)}, u32[]{:S(2)}, u32[]{:S(2)}) async-start(bf16[8,64,1024]{2,1,0:T(8,128)(2,1)} %bitcast.156), calls=%async_computation.2 | async-start | bytes 2097152 | tf_op jit(solution)/shard_map/all_to_all | solution.py:177
Sparse Core Ops, SparseCore 0:
  161.8 37.2 all-reduce.29
  235.5 33.3 all-gather.5
  281.7 44.3 reduce-scatter.1
where the time goes:
time: 371 us; the launch traced here: 370 us
  blocking collectives  155 us (42%)
  waiting for transfers between devices  139 us (37%)
  matrix products  21 us (6%)
  local copies, waits for them, and re-layouts  19.4 us (5%)
  other arithmetic  17.3 us (5%)
  between operations  13.5 us (4%)
  starting transfers between devices  5.77 us (2%)
    all_gather x4, blocking collectives, carried_in(): pieces = jax.tree.map(lambda part: lax.all_gather(part, axis), value)  124 us
    reduce_scatter x1, waiting for transfers between devices, per_device(): lax.psum_scatter(down_part.astype(f32).astype(jnp.bfloat16), 'tp', scatte...  44.6 us
    psum x1, waiting for transfers between devices, per_device(): lax.psum(partial_rows.astype(jnp.bfloat16), 'tp').astype(jnp.float32)  35.4 us
    all_gather x1, waiting for transfers between devices, per_device(): piece = lax.all_gather(arrived, 'tp', axis=2, tiled=True)  33.4 us
    all_to_all x1, blocking collectives, per_device(): lax.all_to_all(dispatch, 'sp', split_axis=0, concat_axis=0, tiled=True)  30.6 us
    all_to_all x1, waiting for transfers between devices, per_device(): lax.all_to_all(expert_out, 'sp', split_axis=0, concat_axis=0, tiled=True)  25.2 us
  transfers between devices with their start and end apart: 4, of which 4 were waited for; matrix products, arithmetic and copies ran while one was open for 1% of the time, Pallas kernels for 0%

commit v1 on v0

--- a/solution.py
+++ b/solution.py
@@ -164,7 +164,8 @@
         experts, capacity, d_local
     )
     arrived = lax.all_to_all(dispatch, "sp", split_axis=0, concat_axis=0, tiled=True)
-    piece = lax.all_gather(arrived, "tp", axis=2, tiled=True)
+    parts = lax.all_gather(arrived, "tp", axis=0, tiled=False)
+    piece = jnp.concatenate(parts, axis=2)
     gate_part = jnp.einsum("snd,df->snf", piece, gate_w, preferred_element_type=f32)
     up_part = jnp.einsum("snd,df->snf", piece, up_w, preferred_element_type=f32)
     hidden = (jax.nn.silu(gate_part) * up_part).astype(bf16)

time: 371 us -> 371 us (level)
  no operation moved by 1% of the time
where the time goes in v1:
time: 371 us; the launch traced here: 370 us
  blocking collectives  155 us (42%)
  waiting for transfers between devices  139 us (37%)
  local copies, waits for them, and re-layouts  22.8 us (6%)
  matrix products  17.4 us (5%)
  other arithmetic  17.3 us (5%)
  between operations  13.5 us (4%)
  starting transfers between devices  5.78 us (2%)
    all_gather x4, blocking collectives, carried_in(): pieces = jax.tree.map(lambda part: lax.all_gather(part, axis), value)  124 us
    reduce_scatter x1, waiting for transfers between devices, per_device(): lax.psum_scatter(down_part.astype(f32).astype(jnp.bfloat16), 'tp', scatte...  44.6 us
    psum x1, waiting for transfers between devices, per_device(): lax.psum(partial_rows.astype(jnp.bfloat16), 'tp').astype(jnp.float32)  35.4 us
    all_gather x1, waiting for transfers between devices, per_device(): parts = lax.all_gather(arrived, 'tp', axis=0, tiled=False)  33.4 us
    all_to_all x1, blocking collectives, per_device(): lax.all_to_all(dispatch, 'sp', split_axis=0, concat_axis=0, tiled=True)  30.6 us
    all_to_all x1, waiting for transfers between devices, per_device(): lax.all_to_all(expert_out, 'sp', split_axis=0, concat_axis=0, tiled=True)  25.2 us
  transfers between devices with their start and end apart: 4, of which 4 were waited for; matrix products, arithmetic and copies ran while one was open for 1% of the time, Pallas kernels for 0%

profile of v1, /device:TPU:0, one launch (start us, length us, event | category | flops | bytes accessed | tf_op | source)
XLA Modules:
  0.0 370.1 jit_solution(10829734964338050824)
XLA Ops:
  8.2 1.6 fusion.45
  9.8 1.6 fusion.49
  23.2 32.4 %all-gather = f32[128,64,1]{1,2,0:T(1,128)S(1)} all-gather(f32[16,64,1]{1,2,0:T(1,128)S(1)} %copy.34), channel_id=2, replica_groups=mesh['sp'=8,'tp'=4] {'sp'}, dimensions={0}, use_global_device_ids=true | all-gather | bytes 36864 | tf_op jit(solution)/shard_map/all_gather | solution.py:12
  57.8 30.5 %all-gather.1 = f32[128,64,1]{1,2,0:T(1,128)S(1)} all-gather(f32[16,64,1]{1,2,0:T(1,128)S(1)} %copy.35), channel_id=3, replica_groups=mesh['sp'=8,'tp'=4] {'sp'}, dimensions={0}, use_global_device_ids=true | all-gather | bytes 36864 | tf_op jit(solution)/shard_map/all_gather | solution.py:12
  88.3 2.0 slice.170
  91.6 30.5 %all-gather.2 = f32[128,64,1]{1,2,0:T(1,128)S(1)} all-gather(f32[16,64,1]{1,2,0:T(1,128)S(1)} %copy.36), channel_id=4, replica_groups=mesh['sp'=8,'tp'=4] {'sp'}, dimensions={0}, use_global_device_ids=true | all-gather | bytes 36864 | tf_op jit(solution)/shard_map/all_gather | solution.py:12
  122.2 2.0 slice.171
  125.4 30.5 %all-gather.3 = f32[128,64,1]{1,2,0:T(1,128)S(1)} all-gather(f32[16,64,1]{1,2,0:T(1,128)S(1)} %copy.37), channel_id=5, replica_groups=mesh['sp'=8,'tp'=4] {'sp'}, dimensions={0}, use_global_device_ids=true | all-gather | bytes 36864 | tf_op jit(solution)/shard_map/all_gather | solution.py:12
  156.4 1.9 fusion.22
  158.2 1.9 fusion.42
  163.7 35.4 %all-reduce.30.cloned.1.call-done = bf16[128,4096]{1,0:T(8,128)(2,1)} async-done(((bf16[128,4096]{1,0:T(8,128)(2,1)}), bf16[128,4096]{1,0:T(8,128)(2,1)}) %all-reduce.30.cloned.1.call-update) | async-done | bytes 1048592 | tf_op jit(solution)/shard_map/psum | solution.py:142
  199.0 1.8 add_convert_fusion
  202.5 2.1 gather_fusion
  204.7 30.6 %all_to_all.10 = bf16[8,64,1024]{2,1,0:T(8,128)(2,1)} all-to-all(bf16[8,64,1024]{2,1,0:T(8,128)(2,1)S(1)} %broadcast_select_fusion), channel_id=1, replica_groups=mesh['sp'=8,'tp'=4] {'sp'}, dimensions={0} | all-to-all | bytes 2097152 | tf_op jit(solution)/shard_map/all_to_all | solution.py:166
  235.4 33.4 %all-gather.7.cloned.1.call-done = bf16[32,64,1024]{2,1,0:T(8,128)(2,1)} async-done(((bf16[8,64,1024]{2,1,0:T(8,128)(2,1)}), bf16[32,64,1024]{2,1,0:T(8,128)(2,1)}) %all-gather.7.cloned.1.call-update) | async-done | bytes 4194320 | tf_op jit(solution)/shard_map/all_gather | solution.py:167
  268.9 2.8 copy.43
  272.3 2.3 fusion.7
  274.7 2.4 fusion.12
  277.1 4.3 %convolution_convert_fusion = bf16[512,4096]{1,0:T(8,128)(2,1)} fusion(bf16[512,512]{1,0:T(8,128)(2,1)S(1)} %bitcast.177, bf16[1,512,4096]{2,1,0:T(8,128)(2,1)S(1)} %copy-done.9), kind=kOutput, calls=%fused_computation.12 | convolution fusion | flops 2149580800 | bytes 8912896 | tf_op jit(solution)/shard_map/dot_general | solution.py:173
  281.4 44.6 %reduce-scatter.2.cloned.1.call-done = bf16[512,1024]{1,0:T(8,128)(2,1)} async-done(((bf16[512,4096]{1,0:T(8,128)(2,1)}), bf16[512,1024]{1,0:T(8,128)(2,1)}) %reduce-scatter.2.cloned.1.call-update) | async-done | bytes 1048592 | tf_op jit(solution)/shard_map/reduce_scatter | solution.py:174
  326.0 5.5 %all-to-all-start.1 = ((bf16[8,64,1024]{2,1,0:T(8,128)(2,1)}), bf16[8,64,1024]{2,1,0:T(8,128)(2,1)S(1)}, u32[]{:S(2)}, u32[]{:S(2)}) async-start(bf16[8,64,1024]{2,1,0:T(8,128)(2,1)} %bitcast.164), calls=%async_computation.2 | async-start | bytes 2097152 | tf_op jit(solution)/shard_map/all_to_all | solution.py:178
  331.9 25.2 %all-to-all-done.1 = bf16[8,64,1024]{2,1,0:T(8,128)(2,1)S(1)} async-done(((bf16[8,64,1024]{2,1,0:T(8,128)(2,1)}), bf16[8,64,1024]{2,1,0:T(8,128)(2,1)S(1)}, u32[]{:S(2)}, u32[]{:S(2)}) %all-to-all-start.1) | async-done | bytes 1048608 | tf_op jit(solution)/shard_map/all_to_all | solution.py:178
  357.2 2.0 gather_fusion.1
  361.8 1.8 add_convert_fusion.1
  (91 shorter events, 27.6 us)
Async XLA Ops:
  6.5 153.6 %copy-start = (bf16[256,4096]{1,0:T(8,128)(2,1)S(1)}, bf16[256,4096]{1,0:T(8,128)(2,1)}, u32[]{:S(2)}) copy-start(bf16[256,4096]{1,0:T(8,128)(2,1)} %param.30) | copy-start | bytes 6291460
  6.5 6.3 %copy-start.3 = (f32[16,128]{1,0:T(8,128)S(1)}, f32[16,128]{1,0:T(8,128)}, u32[]{:S(2)}) copy-start(f32[16,128]{1,0:T(8,128)} %param.29) | copy-start | bytes 24580
  6.5 192.5 %all-reduce.30.cloned.1.call-start = ((), (), s32[]{:S(2)}) async-start(), calls=%async_computation.3 | async-start | bytes 2097152 | tf_op jit(solution)/shard_map/psum | solution.py:142
  20.9 135.3 %copy-start.6 = (f32[256]{0:T(256)S(1)}, f32[256]{0:T(256)}, u32[]{:S(2)}) copy-start(f32[256]{0:T(256)} %param.28) | copy-start | bytes 3076
  21.9 136.3 %copy-start.2 = (bf16[256,128]{1,0:T(8,128)(2,1)S(1)}, bf16[256,128]{1,0:T(8,128)(2,1)}, u32[]{:S(2)}) copy-start(bf16[256,128]{1,0:T(8,128)(2,1)} %param.20) | copy-start | bytes 196612
  156.3 5.6 %copy-start.4 = (s32[128,2]{0,1:T(2,128)S(1)}, s32[128,2]{0,1:T(2,128)}, u32[]{:S(2)}) copy-start(s32[128,2]{0,1:T(2,128)} %param.33) | copy-start | bytes 3076
  161.6 107.2 %all-gather.7.cloned.1.call-start = ((), (), s32[]{:S(2)}) async-start(), calls=%async_computation.5 | async-start | bytes 5242880 | tf_op jit(solution)/shard_map/all_gather | solution.py:167
  163.5 38.9 %dynamic-slice-start = ((f32[4096]{0:T(1024)}, s32[]{:T(128)}), f32[1024]{0:T(1024)S(1)}, s32[]{:S(2)}) async-start(f32[4096]{0:T(1024)} %param.32, s32[]{:T(128)} %select_n.74), calls=%async_computation.6 | async-start | bytes 8704 | tf_op jit(solution)/shard_map/dynamic_slice | solution.py:61
  201.0 1.3 copy-start.1
  235.4 90.6 %reduce-scatter.2.cloned.1.call-start = ((), (), s32[]{:S(2)}) async-start(), calls=%async_computation.4 | async-start | bytes 5242880 | tf_op jit(solution)/shard_map/reduce_scatter | solution.py:174
  268.8 3.4 copy-start.7
  272.3 2.3 copy-start.8
  274.6 2.5 copy-start.9
  281.4 50.4 %copy-start.5 = (f32[128,2]{0,1:T(2,128)S(1)}, f32[128,2]{0,1:T(2,128)}, u32[]{:S(2)}) copy-start(f32[128,2]{0,1:T(2,128)} %param.34) | copy-start | bytes 3076
  326.0 31.2 %all-to-all-start.1 = ((bf16[8,64,1024]{2,1,0:T(8,128)(2,1)}), bf16[8,64,1024]{2,1,0:T(8,128)(2,1)S(1)}, u32[]{:S(2)}, u32[]{:S(2)}) async-start(bf16[8,64,1024]{2,1,0:T(8,128)(2,1)} %bitcast.164), calls=%async_computation.2 | async-start | bytes 2097152 | tf_op jit(solution)/shard_map/all_to_all | solution.py:178
Sparse Core Ops, SparseCore 0:
  161.8 37.2 all-reduce.29
  235.5 33.3 all-gather.6
  281.5 44.3 reduce-scatter.1
